TPU v7x, 32 devices: a whole 2x2x4 slice. The times are simulated.
32 devices in a mesh: sp: 8 (over z, core), tp: 4 (over y, x).
Axes of the slice: x: 2, y: 2, z: 4, core: 2. Of those that a mesh axis runs over, the one named last changes fastest.
Arguments:
- cotangent: bfloat16 [1024, 2048], P('sp'), may hold values from -6 to 6
- mixer_sum: bfloat16 [1024, 2048], P('sp'), may hold values from -180 to 180
- ffn_gain: float32 [2048], replicated, may hold values from 0.1 to 1.9
- expert_ids: int32 [1024, 2], P('sp'), may hold values from 0 to 7, all different within a row; in each aligned block of 128 rows (0 to 127, 128 to 255, ...) at most 40 rows name the same one
- route_weight: float32 [1024, 2], P('sp'), may hold values from 0.1 to 1
- gate_weights: bfloat16 [8, 2048, 2048], P('sp', None, 'tp'), may hold values from -0.125 to 0.125
- up_weights: bfloat16 [8, 2048, 2048], P('sp', None, 'tp'), may hold values from -0.125 to 0.125
- down_weights: bfloat16 [8, 2048, 2048], P('sp', 'tp'), may hold values from -0.125 to 0.125
- out_weight: bfloat16 [2048, 1024], P(None, 'tp'), may hold values from -5 to 5
- conv_output: bfloat16 [1024, 1024], P('sp', 'tp'), may hold values from -6 to 6
- norm_mean: float32 [1024], P('sp'), may hold values from -3 to 3
- norm_rstd: float32 [1024], P('sp'), may hold values from 0.5 to 2
- norm_gain: float32 [1024], P('tp'), may hold values from 0.1 to 1.9
- conv_taps: float32 [31, 1024], P(None, 'tp'), may hold values from -1 to 1
- conv_value: bfloat16 [1024, 1024], P('sp', 'tp'), may hold values from -6 to 6
- conv_gate: bfloat16 [1024, 1024], P('sp', 'tp'), may hold values from -6 to 6
Outputs:
- grad_gate_weights: bfloat16 [8, 2048, 2048], P('sp', None, 'tp')
- grad_up_weights: bfloat16 [8, 2048, 2048], P('sp', None, 'tp')
- grad_down_weights: bfloat16 [8, 2048, 2048], P('sp', 'tp')
- grad_out_weight: float32 [2048, 1024], P('sp', 'tp')
- grad_conv_value: bfloat16 [1024, 1024], P('sp', 'tp')
- grad_conv_gate: bfloat16 [1024, 1024], P('sp', 'tp')
Inputs may be any that keep to these rules, and one draw needn't show every extreme that they name: `expert_ids`: the 2 experts of a row differ. Among the rows of one index of sp no expert is named more than 40 times, and in every draw some index names some expert exactly 40 times.
All inputs are finite; a program needn't handle non-finite values.
Results may differ from a plain program's by a relative error of at most 0.024.
Values may be sent and summed in bfloat16 or wider, within the bound.
A program may use at most 64 MiB of HBM per device.

v0:
```python
import jax
import jax.numpy as jnp
from jax import lax
from jax.sharding import PartitionSpec as P

epsilon = 1e-06


def passed_along(x, axis, by):
    peers = lax.axis_size(axis)
    pairs = [(i, i + by) for i in range(peers) if 0 <= i + by < peers]
    return lax.ppermute(x, axis, pairs)


def slot_layout(route_ids, capacity, expert_count):
    flat_ids = route_ids.reshape(-1)
    onehot = (flat_ids[:, None] == jnp.arange(expert_count, dtype=jnp.int32)[None, :]).astype(
        jnp.int32
    )
    earlier = jnp.cumsum(onehot, axis=0) - onehot
    places = jnp.sum(earlier * onehot, axis=1)
    return flat_ids * capacity + places


def slot_sources(entry_slot, slot_count):
    matches = entry_slot[None, :] == jnp.arange(slot_count, dtype=jnp.int32)[:, None]
    filled = jnp.any(matches, axis=1)
    entries = jnp.arange(entry_slot.shape[0], dtype=jnp.int32)
    sources = jnp.sum(jnp.where(matches, entries[None, :], 0), axis=1)
    return (sources, filled)


def pick_slots(table_rows, sources, filled, per_entry):
    picked = table_rows[sources // per_entry]
    return jnp.where(filled[:, None], picked, jnp.zeros((), table_rows.dtype))


def contract_rows(left, right):
    return lax.dot_general(
        left, right, (((0,), (0,)), ((), ())), preferred_element_type=jnp.float32
    )


def contract_cols(left, right):
    return lax.dot_general(
        left, right, (((1,), (1,)), ((), ())), preferred_element_type=jnp.float32
    )


def local(
    cotangent,
    mixer_sum,
    ffn_gain,
    expert_ids,
    route_weight,
    gate_weights,
    up_weights,
    down_weights,
    out_weight,
    conv_output,
    norm_mean,
    norm_rstd,
    norm_gain,
    conv_taps,
    conv_value,
    conv_gate,
):
    tok_rows, model_width = cotangent.shape
    route_count = expert_ids.shape[1]
    expert_count = lax.axis_size("sp")
    tp_count = lax.axis_size("tp")
    capacity = 5 * route_count * tok_rows // (4 * expert_count)
    feature_share = model_width // tp_count
    feature_start = lax.axis_index("tp") * feature_share
    mixed_float = mixer_sum.astype(jnp.float32)
    row_rstd = lax.rsqrt(jnp.mean(mixed_float * mixed_float, axis=1, keepdims=True) + epsilon)
    mixer_hat = mixed_float * row_rstd
    normed = (mixer_hat * ffn_gain).astype(jnp.bfloat16)
    scaled = (route_weight[:, :, None] * cotangent.astype(jnp.float32)[:, None, :]).astype(
        jnp.bfloat16
    )
    scaled = scaled.reshape(tok_rows * route_count, model_width)
    entry_slot = slot_layout(expert_ids, capacity, expert_count)
    sources, filled = slot_sources(entry_slot, expert_count * capacity)
    normed_part = lax.dynamic_slice_in_dim(normed, feature_start, feature_share, 1)
    scaled_part = lax.dynamic_slice_in_dim(scaled, feature_start, feature_share, 1)
    send_rows = pick_slots(normed_part, sources, filled, route_count).reshape(
        expert_count, capacity, feature_share
    )
    send_cots = pick_slots(scaled_part, sources, filled, 1).reshape(
        expert_count, capacity, feature_share
    )
    rows_part, cots_part = (
        lax.all_to_all(send_rows, "sp", split_axis=0, concat_axis=0, tiled=True),
        lax.all_to_all(send_cots, "sp", split_axis=0, concat_axis=0, tiled=True),
    )
    rows_in, cots_in = (
        lax.all_gather(rows_part, "tp", axis=2, tiled=True),
        lax.all_gather(cots_part, "tp", axis=2, tiled=True),
    )
    expert_rows = rows_in.reshape(-1, model_width)
    expert_cots = cots_in.reshape(-1, model_width)
    gate_mat = gate_weights[0]
    up_mat = up_weights[0]
    down_mat = down_weights[0]
    gate_pre = jnp.dot(expert_rows, gate_mat, preferred_element_type=jnp.float32)
    up_pre = jnp.dot(expert_rows, up_mat, preferred_element_type=jnp.float32)
    gate_sig = jax.nn.sigmoid(gate_pre)
    active = gate_pre * gate_sig
    hidden = (active * up_pre).astype(jnp.bfloat16)
    d_hidden = contract_cols(expert_cots, down_mat)
    d_gate = (d_hidden * up_pre * gate_sig * (1.0 + gate_pre * (1.0 - gate_sig))).astype(
        jnp.bfloat16
    )
    d_up = (d_hidden * active).astype(jnp.bfloat16)
    grad_down = contract_rows(hidden, expert_cots).astype(jnp.bfloat16)
    grad_gate = contract_rows(expert_rows, d_gate).astype(jnp.bfloat16)
    grad_up = contract_rows(expert_rows, d_up).astype(jnp.bfloat16)
    back_rows = contract_cols(d_gate, gate_mat) + contract_cols(d_up, up_mat)
    share_rows = lax.psum_scatter(
        back_rows.astype(jnp.bfloat16), "tp", scatter_dimension=1, tiled=True
    )
    returned_part = lax.all_to_all(
        share_rows.reshape(expert_count, capacity, feature_share),
        "sp",
        split_axis=0,
        concat_axis=0,
        tiled=True,
    )
    returned = lax.all_gather(returned_part, "tp", axis=2, tiled=True)
    picked = returned.reshape(expert_count * capacity, model_width)[entry_slot]
    d_normed = jnp.sum(
        picked.astype(jnp.float32).reshape(tok_rows, route_count, model_width), axis=1
    )
    d_hat = d_normed * ffn_gain
    d_mixed = cotangent.astype(jnp.float32) + row_rstd * (
        d_hat - mixer_hat * jnp.mean(d_hat * mixer_hat, axis=1, keepdims=True)
    )
    d_mixed_b = d_mixed.astype(jnp.bfloat16)
    norm_in = (conv_output.astype(jnp.float32) - norm_mean[:, None]) * norm_rstd[:, None]
    norm_scaled = norm_in * norm_gain
    norm_sig = jax.nn.sigmoid(norm_scaled)
    conv_act = (norm_scaled * norm_sig).astype(jnp.bfloat16)
    grad_out_weight = lax.psum_scatter(
        contract_rows(d_mixed_b, conv_act).astype(jnp.bfloat16),
        "sp",
        scatter_dimension=0,
        tiled=True,
    ).astype(jnp.float32)
    d_act = jnp.dot(d_mixed_b, out_weight, preferred_element_type=jnp.float32)
    d_in = d_act * norm_sig * (1.0 + norm_scaled * (1.0 - norm_sig)) * norm_gain
    channel_total = out_weight.shape[1] * tp_count
    sum_plain, sum_product = lax.psum(
        (jnp.sum(d_in, axis=1), jnp.sum(d_in * norm_in, axis=1)), "tp"
    )
    d_conv = norm_rstd[:, None] * (
        d_in
        - (sum_plain / channel_total)[:, None]
        - norm_in * (sum_product / channel_total)[:, None]
    )
    tap_count = conv_taps.shape[0]
    halo_rows = tap_count - 1
    after_rows = passed_along(d_conv[:halo_rows], "sp", -1)
    extended = jnp.concatenate([d_conv, after_rows], axis=0)
    d_mixin = jnp.zeros_like(d_conv)
    for tap_index in range(tap_count):
        d_mixin = d_mixin + conv_taps[tap_index] * extended[tap_index : tap_index + tok_rows]
    conv_sig = jax.nn.sigmoid(conv_gate.astype(jnp.float32))
    grad_conv_value = (d_mixin * conv_sig).astype(jnp.bfloat16)
    grad_conv_gate = (
        d_mixin * conv_value.astype(jnp.float32) * conv_sig * (1.0 - conv_sig)
    ).astype(jnp.bfloat16)
    return (
        grad_gate[None],
        grad_up[None],
        grad_down[None],
        grad_out_weight,
        grad_conv_value,
        grad_conv_gate,
    )


def solution(mesh):
    return jax.shard_map(
        local,
        mesh=mesh,
        in_specs=(
            P("sp", None),
            P("sp", None),
            P(),
            P("sp", None),
            P("sp", None),
            P("sp", None, "tp"),
            P("sp", None, "tp"),
            P("sp", "tp", None),
            P(None, "tp"),
            P("sp", "tp"),
            P("sp"),
            P("sp"),
            P("tp"),
            P(None, "tp"),
            P("sp", "tp"),
            P("sp", "tp"),
        ),
        out_specs=(
            P("sp", None, "tp"),
            P("sp", None, "tp"),
            P("sp", "tp", None),
            P("sp", "tp"),
            P("sp", "tp"),
            P("sp", "tp"),
        ),
        check_vma=False,
    )
```

profile of v0, /device:TPU:0, one launch (start us, length us, event | category | flops | bytes accessed | tf_op | source)
XLA Modules:
  0.0 237.1 jit_solution(6315690118948202603)
XLA Ops:
  7.2 1.0 copy.26
  8.3 0.1 reshape.191
  8.5 0.6 reduce-window.6
  9.1 0.2 slice_reduce_fusion
  9.4 0.2 select_reduce_fusion
  9.6 0.2 fusion.18
  9.8 1.2 fusion.15
  11.0 2.2 convert_multiply_fusion
  13.2 2.4 %mul.495 = f32[128,2,2048]{2,1,0:T(2,128)} broadcast(bf16[128,2048]{1,0:T(8,128)(2,1)S(1)} %copy-done.3), dimensions={0,2} | broadcast | bytes 2621440 | tf_op jit(solution)/shard_map/mul | solution.py:79
  15.6 3.7 %mul.496 = f32[256,2048]{1,0:T(8,128)} reshape(f32[128,2,2048]{2,1,0:T(2,128)} %mul.495) | data formatting | bytes 4194304 | tf_op jit(solution)/shard_map/mul | solution.py:79
  19.4 0.1 mul.493
  19.7 1.0 fusion.19
  20.7 2.0 gather_fusion
  22.7 1.1 fusion.17
  23.8 2.0 gather_fusion.1
  26.0 17.4 %all_to_all.15 = bf16[8,40,512]{2,1,0:T(8,128)(2,1)} all-to-all(bf16[8,40,512]{2,1,0:T(8,128)(2,1)S(1)} %get-tuple-element.48), channel_id=1, replica_groups=mesh['sp'=8,'tp'=4] {'sp'}, dimensions={0} | all-to-all | bytes 655360 | tf_op jit(solution)/shard_map/all_to_all | solution.py:94
  43.4 14.2 %all_to_all.16 = bf16[8,40,512]{2,1,0:T(8,128)(2,1)} all-to-all(bf16[8,40,512]{2,1,0:T(8,128)(2,1)S(1)} %get-tuple-element.47), channel_id=1, replica_groups=mesh['sp'=8,'tp'=4] {'sp'}, dimensions={0} | all-to-all | bytes 655360 | tf_op jit(solution)/shard_map/all_to_all | solution.py:95
  57.7 13.3 %all-gather.4.cloned.1.call-done = bf16[8,40,2048]{2,1,0:T(8,128)(2,1)} async-done(((bf16[8,40,512]{2,1,0:T(8,128)(2,1)}), bf16[8,40,2048]{2,1,0:T(8,128)(2,1)}) %all-gather.4.cloned.1.call-update) | async-done | bytes 1310736 | tf_op jit(solution)/shard_map/all_gather | solution.py:98
  71.0 2.3 fusion.6
  73.4 1.7 fusion.9
  75.0 26.4 %all-gather.6.cloned.1.call-done = bf16[8,40,2048]{2,1,0:T(8,128)(2,1)} async-done(((bf16[8,40,512]{2,1,0:T(8,128)(2,1)}), bf16[8,40,2048]{2,1,0:T(8,128)(2,1)}) %all-gather.6.cloned.1.call-update) | async-done | bytes 1310736 | tf_op jit(solution)/shard_map/all_gather | solution.py:99
  101.4 3.1 %multiply_convert_fusion.1 = (bf16[320,512]{1,0:T(8,128)(2,1)S(1)}, bf16[320,512]{1,0:T(8,128)(2,1)S(1)}) fusion(f32[320,512]{1,0:T(8,128)S(1)} %fusion.6, f32[320,512]{1,0:T(8,128)} %fusion.9, bf16[320,2048]{1,0:T(8,128)(2,1)} %bitcast.122, bf16[1,512,2048]{2,1,0:T(8,128)(2,1)} %param.23), kind=kOutput, calls=%fused_computation.59 | convolution fusion | flops 673218560 | bytes 5373952 | tf_op jit(solution)/shard_map/dot_general | solution.py:45
  104.6 0.9 fusion.4
  105.5 0.8 copy-done.2
  106.3 1.9 fusion.3
  108.3 29.6 %reduce-scatter.3.cloned.1.call-done = bf16[320,512]{1,0:T(8,128)(2,1)} async-done(((bf16[320,2048]{1,0:T(8,128)(2,1)}), bf16[320,512]{1,0:T(8,128)(2,1)}) %reduce-scatter.3.cloned.1.call-update) | async-done | bytes 327696 | tf_op jit(solution)/shard_map/reduce_scatter | solution.py:120
  137.9 15.8 %all_to_all.17 = bf16[8,40,512]{2,1,0:T(8,128)(2,1)} all-to-all(bf16[8,40,512]{2,1,0:T(8,128)(2,1)} %bitcast.84), channel_id=1, replica_groups=mesh['sp'=8,'tp'=4] {'sp'}, dimensions={0} | all-to-all | bytes 655360 | tf_op jit(solution)/shard_map/all_to_all | solution.py:123
  153.7 0.2 reduce-scatter.5.cloned.1.call-start
  154.3 0.6 fusion.125
  154.9 0.7 fusion.124
  155.6 24.8 %all-gather.8.cloned.1.call-done = bf16[8,40,2048]{2,1,0:T(8,128)(2,1)} async-done(((bf16[8,40,512]{2,1,0:T(8,128)(2,1)}), bf16[8,40,2048]{2,1,0:T(8,128)(2,1)}) %all-gather.8.cloned.1.call-update) | async-done | bytes 1310736 | tf_op jit(solution)/shard_map/all_gather | solution.py:130
  180.4 3.8 %gather_fusion.2 = bf16[256,2048]{1,0:T(8,128)(2,1)S(1)} fusion(bf16[320,2048]{1,0:T(8,128)(2,1)} %bitcast.81, s32[1024]{0:T(1024)S(1)} %pad_clamp_fusion), kind=kCustom, calls=%fused_computation.2 | custom fusion | bytes 2098176 | tf_op jit(solution)/shard_map/gather | solution.py:131
  184.2 2.3 reshape.197
  186.5 4.1 %reduce_sum.72 = f32[128,2048]{1,0:T(8,128)S(1)} reduce(f32[128,2,2048]{2,1,0:T(2,128)} %reshape.197, f32[]{:T(128)} %constant.51.clone.1), dimensions={1}, to_apply=%region_7.8 | reduce | flops 262144 | bytes 3145732 | tf_op jit(solution)/shard_map/reduce_sum | solution.py:132
  190.7 1.4 multiply_reduce_fusion
  192.1 1.6 add_convert_fusion
  193.7 0.8 copy-done.4
  194.6 1.5 convolution_convert_fusion.3
  196.1 4.1 %fusion.1 = bf16[1,2048,512]{2,1,0:T(8,128)(2,1)} fusion(bf16[320,2048]{1,0:T(8,128)(2,1)} %bitcast.119, bf16[320,512]{1,0:T(8,128)(2,1)S(1)} %copy-done.7), kind=kOutput, calls=%fused_computation.8 | convolution fusion | flops 672137216 | bytes 3735552 | tf_op jit(solution)/shard_map/dot_general | solution.py:39
  200.3 2.7 %fusion.2 = bf16[1,512,2048]{2,1,0:T(8,128)(2,1)} fusion(bf16[320,2048]{1,0:T(8,128)(2,1)S(1)} %bitcast.123, f32[320,512]{1,0:T(8,128)S(1)} %copy-done.56, f32[320,512]{1,0:T(8,128)S(1)} %copy-done.55), kind=kOutput, calls=%fused_computation.9 | convolution fusion | flops 673120256 | bytes 4718592 | tf_op jit(solution)/shard_map/dot_general | solution.py:39
  203.0 0.4 fusion.122
  203.4 8.9 %all-reduce = (f32[128]{0:T(128)S(1)}, f32[128]{0:T(128)S(1)}) all-reduce(f32[128]{0:T(128)S(1)} %get-tuple-element.7, f32[128]{0:T(128)S(1)} %get-tuple-element.6), channel_id=1, replica_groups=mesh['sp'=8,'tp'=4] {'tp'}, use_global_device_ids=true, to_apply=%region_13.14 | all-reduce | flops 256 | bytes 2048 | tf_op jit(solution)/shard_map/psum | solution.py:153
  212.8 1.3 collective-permute-start
  214.1 3.9 %fusion = bf16[1,2048,512]{2,1,0:T(8,128)(2,1)} fusion(bf16[320,2048]{1,0:T(8,128)(2,1)} %bitcast.120, bf16[320,512]{1,0:T(8,128)(2,1)S(1)} %get-tuple-element.15), kind=kOutput, calls=%fused_computation.7 | convolution fusion | flops 672137216 | bytes 3735552 | tf_op jit(solution)/shard_map/dot_general | solution.py:39
  218.4 1.1 multiply_convert_fusion.4
  219.4 0.7 multiply_convert_fusion.5
  220.1 8.8 %reduce-scatter.5.cloned.1.call-done = bf16[256,256]{1,0:T(8,128)(2,1)} async-done(((bf16[2048,256]{1,0:T(8,128)(2,1)}), bf16[256,256]{1,0:T(8,128)(2,1)}) %reduce-scatter.5.cloned.1.call-update) | async-done | bytes 131088 | tf_op jit(solution)/shard_map/reduce_scatter | solution.py:144
  229.0 1.6 convert_element_type.95
  (145 shorter events, 1.7 us)
Async XLA Ops:
  7.2 63.9 %copy-start = (bf16[1,2048,512]{2,1,0:T(8,128)(2,1)S(1)}, bf16[1,2048,512]{2,1,0:T(8,128)(2,1)}, u32[]{:S(2)}) copy-start(bf16[1,2048,512]{2,1,0:T(8,128)(2,1)} %param.21) | copy-start | bytes 6291460
  7.2 6.0 %copy-start.3 = (bf16[128,2048]{1,0:T(8,128)(2,1)S(1)}, bf16[128,2048]{1,0:T(8,128)(2,1)}, u32[]{:S(2)}) copy-start(bf16[128,2048]{1,0:T(8,128)(2,1)} %param.16) | copy-start | bytes 1572868
  7.2 63.8 %all-gather.4.cloned.1.call-start = ((), (), s32[]{:S(2)}) async-start(), calls=%async_computation.5 | async-start | bytes 1638400 | tf_op jit(solution)/shard_map/all_gather | solution.py:98
  15.6 4.0 %copy-start.11 = (f32[2048]{0:T(1024)S(1)}, f32[2048]{0:T(1024)}, u32[]{:S(2)}) copy-start(f32[2048]{0:T(1024)} %param.18) | copy-start | bytes 24580
  43.4 58.0 %all-gather.6.cloned.1.call-start = ((), (), s32[]{:S(2)}) async-start(), calls=%async_computation.6 | async-start | bytes 1638400 | tf_op jit(solution)/shard_map/all_gather | solution.py:99
  57.7 80.2 %reduce-scatter.3.cloned.1.call-start = ((), (), s32[]{:S(2)}) async-start(), calls=%async_computation.7 | async-start | bytes 1638400 | tf_op jit(solution)/shard_map/reduce_scatter | solution.py:120
  73.4 28.0 %copy-start.54 = (f32[320,512]{1,0:T(8,128)}, f32[320,512]{1,0:T(8,128)S(1)}, u32[]{:S(2)}) copy-start(f32[320,512]{1,0:T(8,128)S(1)} %fusion.6) | copy-start | bytes 1966084
  108.2 45.7 %copy-start.43 = (s32[128,2]{0,1:T(2,128)S(1)}, s32[128,2]{0,1:T(2,128)}, u32[]{:S(2)}) copy-start(s32[128,2]{0,1:T(2,128)} %param.19) | copy-start | bytes 3076
  108.2 46.0 %copy-start.12 = (f32[31,256]{1,0:T(8,128)S(1)}, f32[31,256]{1,0:T(8,128)}, u32[]{:S(2)}) copy-start(f32[31,256]{1,0:T(8,128)} %param.29) | copy-start | bytes 95236
  108.2 72.1 %all-gather.8.cloned.1.call-start = ((), (), s32[]{:S(2)}) async-start(), calls=%async_computation.8 | async-start | bytes 1638400 | tf_op jit(solution)/shard_map/all_gather | solution.py:130
  153.7 75.2 %reduce-scatter.5.cloned.1.call-start = ((), (), s32[]{:S(2)}) async-start(), calls=%async_computation.9 | async-start | bytes 1179648 | tf_op jit(solution)/shard_map/reduce_scatter | solution.py:144
  190.7 3.9 %copy-start.8 = (bf16[128,256]{1,0:T(8,128)(2,1)S(1)}, bf16[128,256]{1,0:T(8,128)(2,1)}, u32[]{:S(2)}) copy-start(bf16[128,256]{1,0:T(8,128)(2,1)} %param.25) | copy-start | bytes 196612
  196.1 4.1 %copy-start.52 = (bf16[8,40,2048]{2,1,0:T(8,128)(2,1)S(1)}, bf16[8,40,2048]{2,1,0:T(8,128)(2,1)}, u32[]{:S(2)}) copy-start(bf16[8,40,2048]{2,1,0:T(8,128)(2,1)} %all-gather.6.cloned.1.call-done) | copy-start | bytes 3932164
  196.1 4.1 %copy-start.55 = (f32[320,512]{1,0:T(8,128)S(1)}, f32[320,512]{1,0:T(8,128)}, u32[]{:S(2)}) copy-start(f32[320,512]{1,0:T(8,128)} %copy-done.54) | copy-start | bytes 1966084
  196.1 4.1 %copy-start.56 = (f32[320,512]{1,0:T(8,128)S(1)}, f32[320,512]{1,0:T(8,128)}, u32[]{:S(2)}) copy-start(f32[320,512]{1,0:T(8,128)} %fusion.9) | copy-start | bytes 1966084
  212.5 5.6 %copy-start.9 = (bf16[128,256]{1,0:T(8,128)(2,1)S(1)}, bf16[128,256]{1,0:T(8,128)(2,1)}, u32[]{:S(2)}) copy-start(bf16[128,256]{1,0:T(8,128)(2,1)} %param.31) | copy-start | bytes 196612
  212.5 5.6 %copy-start.10 = (bf16[128,256]{1,0:T(8,128)(2,1)S(1)}, bf16[128,256]{1,0:T(8,128)(2,1)}, u32[]{:S(2)}) copy-start(bf16[128,256]{1,0:T(8,128)(2,1)} %param.30) | copy-start | bytes 196612
  212.5 5.6 %copy-start.13 = (f32[1,256]{1,0:T(1,128)S(1)}, f32[1,256]{1,0:T(1,128)}, u32[]{:S(2)}) copy-start(f32[1,256]{1,0:T(1,128)} %get-tuple-element.36) | copy-start | bytes 3076
  212.5 5.6 %copy-start.14 = (f32[1,256]{1,0:T(1,128)S(1)}, f32[1,256]{1,0:T(1,128)}, u32[]{:S(2)}) copy-start(f32[1,256]{1,0:T(1,128)} %get-tuple-element.37) | copy-start | bytes 3076
  212.5 5.6 %copy-start.15 = (f32[1,256]{1,0:T(1,128)S(1)}, f32[1,256]{1,0:T(1,128)}, u32[]{:S(2)}) copy-start(f32[1,256]{1,0:T(1,128)} %get-tuple-element.38) | copy-start | bytes 3076
  212.5 5.6 %copy-start.16 = (f32[1,256]{1,0:T(1,128)S(1)}, f32[1,256]{1,0:T(1,128)}, u32[]{:S(2)}) copy-start(f32[1,256]{1,0:T(1,128)} %get-tuple-element.39) | copy-start | bytes 3076
  212.6 5.6 %copy-start.17 = (f32[1,256]{1,0:T(1,128)S(1)}, f32[1,256]{1,0:T(1,128)}, u32[]{:S(2)}) copy-start(f32[1,256]{1,0:T(1,128)} %get-tuple-element.40) | copy-start | bytes 3076
  212.6 5.6 %copy-start.18 = (f32[1,256]{1,0:T(1,128)S(1)}, f32[1,256]{1,0:T(1,128)}, u32[]{:S(2)}) copy-start(f32[1,256]{1,0:T(1,128)} %get-tuple-element.41) | copy-start | bytes 3076
  212.6 5.6 %copy-start.19 = (f32[1,256]{1,0:T(1,128)S(1)}, f32[1,256]{1,0:T(1,128)}, u32[]{:S(2)}) copy-start(f32[1,256]{1,0:T(1,128)} %get-tuple-element.42) | copy-start | bytes 3076
  212.6 5.6 %copy-start.20 = (f32[1,256]{1,0:T(1,128)S(1)}, f32[1,256]{1,0:T(1,128)}, u32[]{:S(2)}) copy-start(f32[1,256]{1,0:T(1,128)} %get-tuple-element.43) | copy-start | bytes 3076
  212.6 5.6 %copy-start.21 = (f32[1,256]{1,0:T(1,128)S(1)}, f32[1,256]{1,0:T(1,128)}, u32[]{:S(2)}) copy-start(f32[1,256]{1,0:T(1,128)} %get-tuple-element.44) | copy-start | bytes 3076
  212.6 5.6 %copy-start.22 = (f32[1,256]{1,0:T(1,128)S(1)}, f32[1,256]{1,0:T(1,128)}, u32[]{:S(2)}) copy-start(f32[1,256]{1,0:T(1,128)} %get-tuple-element.45) | copy-start | bytes 3076
  212.6 5.6 %copy-start.23 = (f32[1,256]{1,0:T(1,128)S(1)}, f32[1,256]{1,0:T(1,128)}, u32[]{:S(2)}) copy-start(f32[1,256]{1,0:T(1,128)} %get-tuple-element.46) | copy-start | bytes 3076
  212.6 5.6 %copy-start.24 = (f32[1,256]{1,0:T(1,128)S(1)}, f32[1,256]{1,0:T(1,128)}, u32[]{:S(2)}) copy-start(f32[1,256]{1,0:T(1,128)} %get-tuple-element.16) | copy-start | bytes 3076
  212.6 5.6 %copy-start.25 = (f32[1,256]{1,0:T(1,128)S(1)}, f32[1,256]{1,0:T(1,128)}, u32[]{:S(2)}) copy-start(f32[1,256]{1,0:T(1,128)} %get-tuple-element.17) | copy-start | bytes 3076
  212.6 5.6 %copy-start.26 = (f32[1,256]{1,0:T(1,128)S(1)}, f32[1,256]{1,0:T(1,128)}, u32[]{:S(2)}) copy-start(f32[1,256]{1,0:T(1,128)} %get-tuple-element.18) | copy-start | bytes 3076
  212.7 5.6 %copy-start.27 = (f32[1,256]{1,0:T(1,128)S(1)}, f32[1,256]{1,0:T(1,128)}, u32[]{:S(2)}) copy-start(f32[1,256]{1,0:T(1,128)} %get-tuple-element.19) | copy-start | bytes 3076
  212.7 5.6 %copy-start.28 = (f32[1,256]{1,0:T(1,128)S(1)}, f32[1,256]{1,0:T(1,128)}, u32[]{:S(2)}) copy-start(f32[1,256]{1,0:T(1,128)} %get-tuple-element.20) | copy-start | bytes 3076
  212.7 5.6 %copy-start.29 = (f32[1,256]{1,0:T(1,128)S(1)}, f32[1,256]{1,0:T(1,128)}, u32[]{:S(2)}) copy-start(f32[1,256]{1,0:T(1,128)} %get-tuple-element.21) | copy-start | bytes 3076
  212.7 5.6 %copy-start.30 = (f32[1,256]{1,0:T(1,128)S(1)}, f32[1,256]{1,0:T(1,128)}, u32[]{:S(2)}) copy-start(f32[1,256]{1,0:T(1,128)} %get-tuple-element.22) | copy-start | bytes 3076
  212.7 5.6 %copy-start.31 = (f32[1,256]{1,0:T(1,128)S(1)}, f32[1,256]{1,0:T(1,128)}, u32[]{:S(2)}) copy-start(f32[1,256]{1,0:T(1,128)} %get-tuple-element.23) | copy-start | bytes 3076
  212.7 5.6 %copy-start.32 = (f32[1,256]{1,0:T(1,128)S(1)}, f32[1,256]{1,0:T(1,128)}, u32[]{:S(2)}) copy-start(f32[1,256]{1,0:T(1,128)} %get-tuple-element.24) | copy-start | bytes 3076
  212.7 5.6 %copy-start.33 = (f32[1,256]{1,0:T(1,128)S(1)}, f32[1,256]{1,0:T(1,128)}, u32[]{:S(2)}) copy-start(f32[1,256]{1,0:T(1,128)} %get-tuple-element.25) | copy-start | bytes 3076
  212.7 5.6 %copy-start.34 = (f32[1,256]{1,0:T(1,128)S(1)}, f32[1,256]{1,0:T(1,128)}, u32[]{:S(2)}) copy-start(f32[1,256]{1,0:T(1,128)} %get-tuple-element.26) | copy-start | bytes 3076
  212.7 5.6 %copy-start.35 = (f32[1,256]{1,0:T(1,128)S(1)}, f32[1,256]{1,0:T(1,128)}, u32[]{:S(2)}) copy-start(f32[1,256]{1,0:T(1,128)} %get-tuple-element.27) | copy-start | bytes 3076
  212.7 5.6 %copy-start.36 = (f32[1,256]{1,0:T(1,128)S(1)}, f32[1,256]{1,0:T(1,128)}, u32[]{:S(2)}) copy-start(f32[1,256]{1,0:T(1,128)} %get-tuple-element.28) | copy-start | bytes 3076
  212.8 5.6 %copy-start.37 = (f32[1,256]{1,0:T(1,128)S(1)}, f32[1,256]{1,0:T(1,128)}, u32[]{:S(2)}) copy-start(f32[1,256]{1,0:T(1,128)} %get-tuple-element.29) | copy-start | bytes 3076
  212.8 5.6 %copy-start.38 = (f32[1,256]{1,0:T(1,128)S(1)}, f32[1,256]{1,0:T(1,128)}, u32[]{:S(2)}) copy-start(f32[1,256]{1,0:T(1,128)} %get-tuple-element.30) | copy-start | bytes 3076
  212.8 5.6 %copy-start.39 = (f32[1,256]{1,0:T(1,128)S(1)}, f32[1,256]{1,0:T(1,128)}, u32[]{:S(2)}) copy-start(f32[1,256]{1,0:T(1,128)} %get-tuple-element.31) | copy-start | bytes 3076
  212.8 5.6 %copy-start.40 = (f32[1,256]{1,0:T(1,128)S(1)}, f32[1,256]{1,0:T(1,128)}, u32[]{:S(2)}) copy-start(f32[1,256]{1,0:T(1,128)} %get-tuple-element.32) | copy-start | bytes 3076
  212.8 5.6 %copy-start.41 = (f32[1,256]{1,0:T(1,128)S(1)}, f32[1,256]{1,0:T(1,128)}, u32[]{:S(2)}) copy-start(f32[1,256]{1,0:T(1,128)} %get-tuple-element.33) | copy-start | bytes 3076
  212.8 5.6 %copy-start.42 = (f32[1,256]{1,0:T(1,128)S(1)}, f32[1,256]{1,0:T(1,128)}, u32[]{:S(2)}) copy-start(f32[1,256]{1,0:T(1,128)} %get-tuple-element.34) | copy-start | bytes 3076
  212.8 5.2 %collective-permute-start = (f32[30,256]{1,0:T(8,128)S(1)}, f32[30,256]{1,0:T(8,128)S(1)}, u32[]{:S(2)}, u32[]{:S(2)}) collective-permute-start(f32[30,256]{1,0:T(8,128)S(1)} %slice.263), channel_id=1, source_target_pairs={{4,0},{8,4},{12,8},{16,12},{20,16},{24,20},{28,24},{5,1},{9,5},{13... | collective-permute-start | bytes 92168 | tf_op jit(solution)/shard_map/ppermute | solution.py:12
  (15 other events, 38.4 us)
Sparse Core Ops, SparseCore 0:
  43.5 27.4 all-gather.3
  72.8 28.5 all-gather.5
  108.4 29.4 reduce-scatter.2
  153.8 26.4 all-gather.7
  196.2 32.6 reduce-scatter.4
where the time goes:
time: 238 us; the launch traced here: 237 us
  waiting for transfers between devices  103 us (43%)
  blocking collectives  56.3 us (24%)
  matrix products  22.5 us (9%)
  local copies, waits for them, and re-layouts  21.6 us (9%)
  other arithmetic  17.3 us (7%)
  between operations  14.7 us (6%)
    reduce_scatter x1, waiting for transfers between devices, local(): lax.psum_scatter(back_rows.astype(jnp.bfloat16), 'tp', scatter_dimension=...  29.6 us
    all_gather x1, waiting for transfers between devices, local(): lax.all_gather(cots_part, 'tp', axis=2, tiled=True)  26.4 us
    all_gather x1, waiting for transfers between devices, local(): returned = lax.all_gather(returned_part, 'tp', axis=2, tiled=True)  24.8 us
    all_to_all x1, blocking collectives, local(): lax.all_to_all(send_rows, 'sp', split_axis=0, concat_axis=0, tiled=True)  17.4 us
    all_to_all x1, blocking collectives, local(): lax.all_to_all(share_rows.reshape(expert_count, capacity, feature_share),...  15.8 us
    all_to_all x1, blocking collectives, local(): lax.all_to_all(send_cots, 'sp', split_axis=0, concat_axis=0, tiled=True)  14.2 us
    all_gather x1, waiting for transfers between devices, local(): lax.all_gather(rows_part, 'tp', axis=2, tiled=True)  13.3 us
    dot_general x4, matrix products, contract_rows(): lax.dot_general(left, right, (((0,), (0,)), ((), ())), preferred_element_...  12.2 us
  transfers between devices with their start and end apart: 6, of which 5 were waited for; matrix products, arithmetic and copies ran while one was open for 8% of the time, Pallas kernels for 0%

commit v1 on v0

v1 whole, which is shorter than its diff:
```python
import functools

import jax
import jax.numpy as jnp
from jax import lax
from jax.experimental import pallas as pl
from jax.experimental.pallas import tpu as pltpu
from jax.sharding import PartitionSpec as P

epsilon = 1e-06
MESH = pl.DeviceIdType.MESH
f32 = jnp.float32
bf16 = jnp.bfloat16


def contract_rows(left, right):
    return lax.dot_general(left, right, (((0,), (0,)), ((), ())), preferred_element_type=f32)


def contract_cols(left, right):
    return lax.dot_general(left, right, (((1,), (1,)), ((), ())), preferred_element_type=f32)


def loop(count, body):
    if count <= 8:
        for i in range(count):
            body(i)
    else:
        def step(i, carry):
            body(i)
            return carry
        lax.fori_loop(0, count, step, 0)


def remote(src, dst, send, recv, sp, tp):
    return pltpu.make_async_remote_copy(
        src_ref=src, dst_ref=dst, send_sem=send, recv_sem=recv,
        device_id={"sp": sp, "tp": tp}, device_id_type=MESH,
    )


def greet(sps, tps, sp, tp):
    barrier = pltpu.get_barrier_semaphore()

    def over_sp(d):
        pl.semaphore_signal(barrier, inc=1, device_id={"sp": (sp + d + 1) % sps, "tp": tp}, device_id_type=MESH)

    def over_tp(d):
        pl.semaphore_signal(barrier, inc=1, device_id={"sp": sp, "tp": (tp + d + 1) % tps}, device_id_type=MESH)

    loop(sps - 1, over_sp)
    loop(tps - 1, over_tp)
    pl.semaphore_wait(barrier, sps + tps - 2)


def dispatch_kernel(sps, tps, in_ref, out_ref, loc_sem, send_a, send_b, recv):
    sp, tp = lax.axis_index("sp"), lax.axis_index("tp")
    width = in_ref.shape[-1]

    def spot(s, t):
        return out_ref.at[:, s, :, pl.ds(pl.multiple_of(t * width, width), width)]

    own = pltpu.make_async_copy(in_ref.at[:, sp], spot(sp, tp), loc_sem)
    own.start()
    greet(sps, tps, sp, tp)

    def first(d, wait=False):
        to = (sp + d + 1) % sps
        copy = remote(in_ref.at[:, to], spot(sp, tp), send_a.at[d], recv.at[sp, tp], to, tp)
        copy.wait_send() if wait else copy.start()

    loop(sps - 1, first)

    def got(s, t):
        remote(spot(s, t), spot(s, t), send_a.at[0], recv.at[s, t], (sp + 1) % sps, tp).wait_recv()

    own.wait()
    if tps == 4:
        x, y = tp % 2, tp // 2
        xn, yn = y * 2 + (1 - x), (1 - y) * 2 + x
        diag = 3 - tp

        def direct(d, wait=False):
            s = (sp + sps - d) % sps
            for k, to in enumerate((xn, yn)):
                copy = remote(spot(s, tp), spot(s, tp), send_b.at[s, k], recv.at[s, tp], sp, to)
                copy.wait_send() if wait else copy.start()

        def relay(d, wait=False):
            s = (sp + sps - d) % sps
            odd = d % 2
            held = xn if odd == 0 else yn
            to = yn if odd == 0 else xn
            if not wait:
                got(s, held)
            copy = remote(spot(s, held), spot(s, held), send_b.at[s, 2], recv.at[s, held], sp, to)
            copy.wait_send() if wait else copy.start()
            if not wait:
                got(s, yn if odd == 0 else xn)

        assert sps <= 8
        direct(0)
        for d in range(1, sps):
            got((sp + sps - d) % sps, tp)
            direct(d)
            relay(d - 1)
        relay(sps - 1)
        for d in range(sps):
            got((sp + sps - d) % sps, diag)
        for d in range(sps):
            direct(d, True)
            relay(d, True)
    else:
        def spread(d, wait=False):
            s = (sp + sps - d) % sps

            def one(k):
                copy = remote(spot(s, tp), spot(s, tp), send_b.at[s, k], recv.at[s, tp], sp, (tp + k + 1) % tps)
                copy.wait_send() if wait else copy.start()

            loop(tps - 1, one)

        spread(0)

        def later(d):
            got((sp + sps - d - 1) % sps, tp)
            spread(d + 1)

        loop(sps - 1, later)
        loop(sps, lambda s: loop(tps - 1, lambda k: got(s, (tp + k + 1) % tps)))
        loop(sps, lambda d: spread(d, True))
    loop(sps - 1, lambda d: first(d, True))


def dispatch(send, sps, tps):
    parts, _, cap, width = send.shape
    return pl.pallas_call(
        functools.partial(dispatch_kernel, sps, tps),
        out_shape=jax.ShapeDtypeStruct((parts, sps, cap, width * tps), send.dtype),
        in_specs=[pl.BlockSpec(memory_space=pltpu.VMEM)],
        out_specs=pl.BlockSpec(memory_space=pltpu.VMEM),
        scratch_shapes=[
            pltpu.SemaphoreType.DMA,
            pltpu.SemaphoreType.DMA((sps,)),
            pltpu.SemaphoreType.DMA((sps, tps)),
            pltpu.SemaphoreType.DMA((sps, tps)),
        ],
        compiler_params=pltpu.CompilerParams(collective_id=0, has_side_effects=True),
        name="dispatch",
    )(send)


def combine_kernel(sps, tps, back_ref, comb_ref, act_ref, dn_ref, acts_ref, stage, sums, ret, total, part,
                   loc_sem, send_c, recv_c, send_r, recv_r, send_a, recv_a, send_g, recv_g):
    sp, tp = lax.axis_index("sp"), lax.axis_index("tp")
    width = ret.shape[-1]

    def cols(ref, t):
        return ref.at[:, pl.ds(pl.multiple_of(t * width, width), width)]

    own = pltpu.make_async_copy(act_ref, acts_ref.at[sp], loc_sem)
    own.start()
    greet(sps, tps, sp, tp)

    def reduce_send(d, wait=False):
        s = (sp + d + 1) % sps

        def one(k):
            to = (tp + k + 1) % tps
            copy = remote(cols(back_ref.at[s], to), stage.at[tp, s], send_r.at[s, k], recv_r.at[tp, s], sp, to)
            copy.wait_send() if wait else copy.start()

        loop(tps - 1, one)

    loop(sps, reduce_send)

    def act_send(d, wait=False):
        to = (sp + d + 1) % sps
        copy = remote(act_ref, acts_ref.at[sp], send_c.at[d], recv_c.at[sp], to, tp)
        copy.wait_send() if wait else copy.start()

    loop(sps - 1, act_send)

    def reduced(s):
        def take(k):
            t = (tp + k + 1) % tps
            remote(stage.at[t, s], stage.at[t, s], send_r.at[0, 0], recv_r.at[t, s], sp, t).wait_recv()

        loop(tps - 1, take)
        value = back_ref[s, :, pl.ds(pl.multiple_of(tp * width, width), width)].astype(f32)
        for k in range(tps - 1):
            value = value + stage[(tp + k + 1) % tps, s].astype(f32)
        return value.astype(bf16)

    def turn(d, wait=False):
        s = (sp + d + 1) % sps
        if not wait:
            sums[s] = reduced(s)
        copy = remote(sums.at[s], ret.at[sp], send_a.at[d], recv_a.at[sp], s, tp)
        copy.wait_send() if wait else copy.start()

    loop(sps - 1, turn)
    total[...] = jnp.dot(comb_ref[sp], reduced(sp), preferred_element_type=f32)

    def add(d):
        s = (sp + sps - d - 1) % sps
        remote(ret.at[s], ret.at[s], send_a.at[0], recv_a.at[s], s, tp).wait_recv()
        total[...] += jnp.dot(comb_ref[s], ret[s], preferred_element_type=f32)

    loop(sps - 1, add)
    part[...] = total[...].astype(bf16)

    def gather(k, wait=False):
        to = (tp + k + 1) % tps
        copy = remote(part, cols(dn_ref, tp), send_g.at[k], recv_g.at[tp], sp, to)
        copy.wait_send() if wait else copy.start()

    loop(tps - 1, gather)
    dn_ref[:, pl.ds(pl.multiple_of(tp * width, width), width)] = total[...].astype(bf16)

    def gathered(k):
        t = (tp + k + 1) % tps
        remote(part, cols(dn_ref, t), send_g.at[0], recv_g.at[t], sp, t).wait_recv()

    loop(tps - 1, gathered)

    def act_take(d):
        s = (sp + sps - d - 1) % sps
        remote(act_ref, acts_ref.at[s], send_c.at[0], recv_c.at[s], s, tp).wait_recv()

    loop(sps - 1, act_take)
    own.wait()
    loop(sps, lambda d: reduce_send(d, True))
    loop(sps - 1, lambda d: act_send(d, True))
    loop(sps - 1, lambda d: turn(d, True))
    loop(tps - 1, lambda k: gather(k, True))


def combine(back, comb, act, sps, tps):
    _, cap, model = back.shape
    tok, channels = act.shape
    width = model // tps
    dma = pltpu.SemaphoreType.DMA
    vm = pl.BlockSpec(memory_space=pltpu.VMEM)
    return pl.pallas_call(
        functools.partial(combine_kernel, sps, tps),
        out_shape=(
            jax.ShapeDtypeStruct((tok, model), bf16),
            jax.ShapeDtypeStruct((sps, tok, channels), bf16),
        ),
        in_specs=[vm] * 3,
        out_specs=(vm, vm),
        scratch_shapes=[
            pltpu.VMEM((tps, sps, cap, width), bf16),
            pltpu.VMEM((sps, cap, width), bf16),
            pltpu.VMEM((sps, cap, width), bf16),
            pltpu.VMEM((tok, width), f32),
            pltpu.VMEM((tok, width), bf16),
            dma,
            dma((sps,)),
            dma((sps,)),
            dma((sps, tps)),
            dma((tps, sps)),
            dma((sps,)),
            dma((sps,)),
            dma((tps,)),
            dma((tps,)),
        ],
        compiler_params=pltpu.CompilerParams(collective_id=1, has_side_effects=True),
        name="combine",
    )(back, comb, act)


def finish_kernel(sps, tps, halo, dm_ref, d_in_ref, norm_in_ref, rstd_ref, taps_ref, all_ref, mix_ref,
                  ext, part, parts, loc_sem, send_m, recv_m, send_s, recv_s, send_h, recv_h):
    sp, tp = lax.axis_index("sp"), lax.axis_index("tp")
    tok = d_in_ref.shape[0]
    channel_total = d_in_ref.shape[1] * tps
    own = pltpu.make_async_copy(dm_ref.at[sp], all_ref.at[sp], loc_sem)
    own.start()
    d_in = d_in_ref[...]
    norm_in = norm_in_ref[...]
    lane = lax.broadcasted_iota(jnp.int32, (tok, 128), 1)
    plain = jnp.sum(d_in, axis=1, keepdims=True)
    product = jnp.sum(d_in * norm_in, axis=1, keepdims=True)
    packed = jnp.where(lane == 0, plain, jnp.where(lane == 1, product, 0.0))
    mine = jnp.transpose(packed)[0:8]
    part[...] = mine
    greet(sps, tps, sp, tp)

    def sums_send(k, wait=False):
        to = (tp + k + 1) % tps
        copy = remote(part, parts.at[tp], send_s.at[k], recv_s.at[tp], sp, to)
        copy.wait_send() if wait else copy.start()

    loop(tps - 1, sums_send)

    def rows_send(d, wait=False):
        to = (sp + d + 1) % sps
        copy = remote(dm_ref.at[to], all_ref.at[sp], send_m.at[d], recv_m.at[sp], to, tp)
        copy.wait_send() if wait else copy.start()

    both = mine
    for k in range(tps - 1):
        t = (tp + k + 1) % tps
        remote(part, parts.at[t], send_s.at[0], recv_s.at[t], sp, t).wait_recv()
        both = both + parts[t]
    wide = jnp.transpose(jnp.concatenate([both] * 16, axis=0))
    plain = wide[:, 0:1] / channel_total
    product = wide[:, 1:2] / channel_total
    ext[0:tok, :] = rstd_ref[...] * (d_in - plain - norm_in * product)

    def halo_copy():
        return remote(ext.at[0:halo], ext.at[tok:tok + halo], send_h, recv_h, (sp + sps - 1) % sps, tp)

    @pl.when(sp > 0)
    def _():
        halo_copy().start()

    loop(sps - 1, rows_send)

    @pl.when(sp < sps - 1)
    def _():
        halo_copy().wait_recv()

    @pl.when(sp == sps - 1)
    def _():
        ext[tok:tok + halo, :] = jnp.zeros((halo, ext.shape[1]), f32)

    taps = taps_ref.shape[0]
    step = 32
    for base in range(0, tok, step):
        acc = taps_ref[0:1, :] * ext[base:base + step, :]
        for j in range(1, taps):
            acc = acc + taps_ref[j:j + 1, :] * ext[base + j:base + j + step, :]
        mix_ref[base:base + step, :] = acc

    def rows_take(d):
        s = (sp + sps - d - 1) % sps
        remote(dm_ref.at[s], all_ref.at[s], send_m.at[0], recv_m.at[s], s, tp).wait_recv()

    loop(sps - 1, rows_take)
    own.wait()

    @pl.when(sp > 0)
    def _():
        halo_copy().wait_send()

    loop(tps - 1, lambda k: sums_send(k, True))
    loop(sps - 1, lambda d: rows_send(d, True))


def finish(dm, d_in, norm_in, rstd, taps, sps, tps):
    tok, channels = d_in.shape
    halo = (taps.shape[0] + 7) // 8 * 8
    dma = pltpu.SemaphoreType.DMA
    vm = pl.BlockSpec(memory_space=pltpu.VMEM)
    return pl.pallas_call(
        functools.partial(finish_kernel, sps, tps, halo),
        out_shape=(
            jax.ShapeDtypeStruct(dm.shape, bf16),
            jax.ShapeDtypeStruct((tok, channels), f32),
        ),
        in_specs=[vm] * 5,
        out_specs=(vm, vm),
        scratch_shapes=[
            pltpu.VMEM((tok + halo, channels), f32),
            pltpu.VMEM((8, tok), f32),
            pltpu.VMEM((tps, 8, tok), f32),
            dma,
            dma((sps,)),
            dma((sps,)),
            dma((tps,)),
            dma((tps,)),
            dma,
            dma,
        ],
        compiler_params=pltpu.CompilerParams(collective_id=2, has_side_effects=True),
        name="finish",
    )(dm, d_in, norm_in, rstd, taps)


def local(
    cotangent,
    mixer_sum,
    ffn_gain,
    expert_ids,
    route_weight,
    gate_weights,
    up_weights,
    down_weights,
    out_weight,
    conv_output,
    norm_mean,
    norm_rstd,
    norm_gain,
    conv_taps,
    conv_value,
    conv_gate,
):
    tok_rows, model_width = cotangent.shape
    route_count = expert_ids.shape[1]
    sps = lax.axis_size("sp")
    tps = lax.axis_size("tp")
    capacity = 5 * route_count * tok_rows // (4 * sps)
    feature_share = model_width // tps
    feature_start = lax.axis_index("tp") * feature_share
    mixed_float = mixer_sum.astype(f32)
    row_rstd = lax.rsqrt(jnp.mean(mixed_float * mixed_float, axis=1, keepdims=True) + epsilon)
    mixer_hat = mixed_float * row_rstd

    experts = jnp.arange(sps, dtype=jnp.int32)
    named = [expert_ids[:, k][:, None] == experts[None, :] for k in range(route_count)]
    onehot = sum(n.astype(bf16) for n in named)
    order = jnp.arange(tok_rows, dtype=jnp.int32)
    lower = (order[:, None] > order[None, :]).astype(bf16)
    earlier = jnp.dot(lower, onehot, preferred_element_type=f32).astype(jnp.int32)
    place = jnp.where(onehot > 0, earlier, -1)
    weight = sum(jnp.where(named[k], route_weight[:, k][:, None], 0.0) for k in range(route_count))
    caps = jnp.arange(capacity, dtype=jnp.int32)
    place_t, weight_t = place.T, weight.T
    pick = place_t[:, None, :] == caps[None, :, None]
    slot_weight = jnp.sum(jnp.where(pick, weight_t[:, None, :], 0.0), axis=2)
    pick_b = pick.astype(bf16)
    comb = (place_t[:, :, None] == caps[None, None, :]).astype(bf16)

    mixer_part = lax.dynamic_slice_in_dim(mixer_sum, feature_start, feature_share, 1)
    gain_part = lax.dynamic_slice_in_dim(ffn_gain, feature_start, feature_share, 0)
    normed_part = (mixer_part.astype(f32) * row_rstd * gain_part).astype(bf16)
    cot_part = lax.dynamic_slice_in_dim(cotangent, feature_start, feature_share, 1)
    picks = pick_b.reshape(sps * capacity, tok_rows)
    picked = jnp.dot(picks, jnp.concatenate([normed_part, cot_part], axis=1), preferred_element_type=f32)
    send = jnp.stack([
        picked[:, :feature_share].astype(bf16),
        (picked[:, feature_share:] * slot_weight.reshape(-1)[:, None]).astype(bf16),
    ]).reshape(2, sps, capacity, feature_share)

    rows_all = dispatch(send, sps, tps)
    expert_rows = rows_all[0].reshape(-1, model_width)
    expert_cots = rows_all[1].reshape(-1, model_width)
    gate_mat = gate_weights[0]
    up_mat = up_weights[0]
    down_mat = down_weights[0]
    gate_pre = jnp.dot(expert_rows, gate_mat, preferred_element_type=f32)
    up_pre = jnp.dot(expert_rows, up_mat, preferred_element_type=f32)
    gate_sig = jax.nn.sigmoid(gate_pre)
    active = gate_pre * gate_sig
    hidden = (active * up_pre).astype(bf16)
    d_hidden = contract_cols(expert_cots, down_mat)
    d_gate = (d_hidden * up_pre * gate_sig * (1.0 + gate_pre * (1.0 - gate_sig))).astype(bf16)
    d_up = (d_hidden * active).astype(bf16)
    grad_down = contract_rows(hidden, expert_cots).astype(bf16)
    grad_gate = contract_rows(expert_rows, d_gate).astype(bf16)
    grad_up = contract_rows(expert_rows, d_up).astype(bf16)
    back_rows = (contract_cols(d_gate, gate_mat) + contract_cols(d_up, up_mat)).astype(bf16)

    norm_in = (conv_output.astype(f32) - norm_mean[:, None]) * norm_rstd[:, None]
    norm_scaled = norm_in * norm_gain
    norm_sig = jax.nn.sigmoid(norm_scaled)
    conv_act = (norm_scaled * norm_sig).astype(bf16)

    d_normed, acts_all = combine(back_rows.reshape(sps, capacity, model_width), comb, conv_act, sps, tps)
    d_hat = d_normed.astype(f32) * ffn_gain
    d_mixed = cotangent.astype(f32) + row_rstd * (
        d_hat - mixer_hat * jnp.mean(d_hat * mixer_hat, axis=1, keepdims=True)
    )
    d_mixed_b = d_mixed.astype(bf16)
    d_act = jnp.dot(d_mixed_b, out_weight, preferred_element_type=f32)
    d_in = d_act * norm_sig * (1.0 + norm_scaled * (1.0 - norm_sig)) * norm_gain
    blocks = d_mixed_b.reshape(tok_rows, sps, model_width // sps).transpose(1, 0, 2)
    dm_all, d_mixin = finish(blocks, d_in, norm_in, norm_rstd[:, None], conv_taps, sps, tps)
    grad_out_weight = contract_rows(
        dm_all.reshape(sps * tok_rows, -1), acts_all.reshape(sps * tok_rows, -1)
    )
    conv_sig = jax.nn.sigmoid(conv_gate.astype(f32))
    grad_conv_value = (d_mixin * conv_sig).astype(bf16)
    grad_conv_gate = (d_mixin * conv_value.astype(f32) * conv_sig * (1.0 - conv_sig)).astype(bf16)
    return (
        grad_gate[None],
        grad_up[None],
        grad_down[None],
        grad_out_weight,
        grad_conv_value,
        grad_conv_gate,
    )


def solution(mesh):
    return jax.shard_map(
        local,
        mesh=mesh,
        in_specs=(
            P("sp", None),
            P("sp", None),
            P(),
            P("sp", None),
            P("sp", None),
            P("sp", None, "tp"),
            P("sp", None, "tp"),
            P("sp", "tp", None),
            P(None, "tp"),
            P("sp", "tp"),
            P("sp"),
            P("sp"),
            P("tp"),
            P(None, "tp"),
            P("sp", "tp"),
            P("sp", "tp"),
        ),
        out_specs=(
            P("sp", None, "tp"),
            P("sp", None, "tp"),
            P("sp", "tp", None),
            P("sp", "tp"),
            P("sp", "tp"),
            P("sp", "tp"),
        ),
        check_vma=False,
    )
```

time: 238 us -> 134 us (0.56)
  waiting for transfers between devices: 103 us -> 0 us
  Pallas kernels: 0 us -> 90.2 us
  blocking collectives: 56.3 us -> 0 us
  between operations: 14.7 us -> 0.93 us
  local copies, waits for them, and re-layouts: 21.6 us -> 10.9 us
  other arithmetic: 17.3 us -> 9.78 us
    pallas_call x0 -> x3, Pallas kernels: none -> 90.2 us  [the longest x1 36.9 us: dispatch(): pl.pallas_call(functools.partial(dispatch_kernel, sps, tps), out_shape=ja...]
    all_gather x3 -> x0, waiting for transfers between devices: 64.5 us -> none  [the longest x1 26.4 us: local(): lax.all_gather(cots_part, 'tp', axis=2, tiled=True)]
    all_to_all x3 -> x0, blocking collectives: 47.4 us -> none  [the longest x1 17.4 us: local(): lax.all_to_all(send_rows, 'sp', split_axis=0, concat_axis=0, tiled=True)]
    reduce_scatter x2 -> x0, waiting for transfers between devices: 38.4 us -> none  [the longest x1 29.6 us: local(): lax.psum_scatter(back_rows.astype(jnp.bfloat16), 'tp', scatter_dimension=...]
    psum x1 -> x0, blocking collectives: 8.94 us -> none  [local(): lax.psum((jnp.sum(d_in, axis=1), jnp.sum(d_in * norm_in, axis=1)), 'tp')]
    gather x3 -> x0, local copies, waits for them, and re-layouts: 7.89 us -> none  [the longest x2 4.05 us: pick_slots(): picked = table_rows[sources // per_entry]]
    mul x5 -> x1, local copies, waits for them, and re-layouts: 6.43 us -> 0.08 us  [local(): picked[:, feature_share:] * slot_weight.reshape(-1)[:, None]]
    reduce_sum x3 -> x1, other arithmetic: 4.37 us -> 0.11 us  [local(): slot_weight = jnp.sum(jnp.where(pick, weight_t[:, None, :], 0.0), axis=2)]
  transfers between devices with their start and end apart: 6 -> 0, of which waited for: 5 -> 0; matrix products, arithmetic and copies ran while one was open for 8% -> 0% of each run, Pallas kernels for 0% -> 0%
where the time goes in v1:
time: 134 us; the launch traced here: 132 us
  Pallas kernels  90.2 us (67%)
  matrix products  20.7 us (15%)
  local copies, waits for them, and re-layouts  10.9 us (8%)
  other arithmetic  9.78 us (7%)
    pallas_call x1, Pallas kernels, dispatch(): pl.pallas_call(functools.partial(dispatch_kernel, sps, tps), out_shape=ja...  36.9 us
    pallas_call x1, Pallas kernels, combine(): pl.pallas_call(functools.partial(combine_kernel, sps, tps), out_shape=(ja...  34.2 us
    pallas_call x1, Pallas kernels, finish(): pl.pallas_call(functools.partial(finish_kernel, sps, tps, halo), out_shap...  19 us
    dot_general x4, matrix products, contract_rows(): lax.dot_general(left, right, (((0,), (0,)), ((), ())), preferred_element_...  11.5 us
    dot_general x3, matrix products, contract_cols(): lax.dot_general(left, right, (((1,), (1,)), ((), ())), preferred_element_...  3.84 us
    unnamed x42, local copies, waits for them, and re-layouts  2.73 us

profile of v1, /device:TPU:0, one launch (start us, length us, event | category | flops | bytes accessed | tf_op | source)
XLA Modules:
  0.0 132.4 jit_solution(15640795280852714997)
XLA Ops:
  0.6 0.0 copy-start
  0.7 0.9 dynamic_slice.10
  1.6 1.2 fusion.23
  2.8 1.0 multiply_convert_fusion.4
  3.8 1.6 %constant_dynamic-slice_fusion = bf16[128,512]{1,0:T(8,128)(2,1)} fusion(bf16[128,2048]{1,0:T(8,128)(2,1)} %param.16, s32[]{:T(128)S(6)} %select_n.32), kind=kLoop, calls=%fused_computation.76 | loop fusion | bytes 262148 | tf_op jit(solution)/shard_map/dynamic_slice | solution.py:430
  5.4 0.8 slice_bitcast_fusion.3
  6.1 0.1 fusion.17
  6.3 0.1 eq.108
  6.4 0.1 bitcast_compare_fusion
  6.5 1.2 fusion.27
  7.7 0.8 slice_bitcast_fusion.1
  8.5 0.1 select_reduce_fusion
  8.6 0.1 mul.138
  8.7 0.1 fusion.24
  8.9 0.9 pad_maximum_fusion.in_ref
  9.8 36.9 %dispatch.1 = bf16[2,8,40,2048]{3,2,1,0:T(8,128)(2,1)} custom-call(bf16[2,8,40,512]{3,2,1,0:T(8,128)(2,1)} %pad_maximum_fusion.in_ref), custom_call_target="tpu_custom_call" | custom-call | tf_op jit(solution)/shard_map/dispatch/pallas_call | solution.py:137
  46.7 1.9 %fusion.44 = (bf16[1,8,40,2048]{3,2,1,0:T(8,128)(2,1)S(1)}, bf16[1,8,40,2048]{3,2,1,0:T(8,128)(2,1)S(1)}) fusion(bf16[2,8,40,2048]{3,2,1,0:T(8,128)(2,1)} %dispatch.1), kind=kLoop, calls=%fused_computation.82 | loop fusion | bytes 5242880 | tf_op jit(solution)/shard_map/slice | solution.py:440
  48.6 0.0 copy-start.3
  48.6 0.0 copy-start.5
  48.6 0.0 copy-start.2
  48.6 0.9 fusion.6
  49.5 0.2 copy-done.3
  49.6 1.5 %copy-done.2 = bf16[1,2048,512]{2,1,0:T(8,128)(2,1)S(1)} copy-done((bf16[1,2048,512]{2,1,0:T(8,128)(2,1)S(1)}, bf16[1,2048,512]{2,1,0:T(8,128)(2,1)}, u32[]{:S(2)}) %copy-start.2) | copy-done | bytes 2097176
  51.1 0.8 fusion.9
  52.0 0.0 copy-start.20
  52.0 1.0 copy-done.18
  53.0 1.0 multiply_convert_fusion.1
  54.1 0.9 fusion.4
  55.0 0.0 copy-start.11
  55.0 0.0 copy-start.15
  55.0 0.0 copy-start.16
  55.0 0.0 copy-start.17
  55.0 1.9 %fusion.3 = bf16[320,2048]{1,0:T(8,128)(2,1)} fusion(f32[320,2048]{1,0:T(8,128)S(1)} %fusion.4, bf16[320,512]{1,0:T(8,128)(2,1)S(1)} %get-tuple-element.16, bf16[1,2048,512]{2,1,0:T(8,128)(2,1)S(1)} %copy-done.2), kind=kOutput, calls=%fused_computation.7 | convolution fusion | flops 672399360 | bytes 6356992 | tf_op jit(solution)/shard_map/dot_general | solution.py:21
  57.0 0.9 fusion.26.comb_ref
  57.9 0.8 subtract_multiply_fusion
  58.7 34.2 %combine.1 = (bf16[128,2048]{1,0:T(8,128)(2,1)}, bf16[8,128,256]{2,1,0:T(8,128)(2,1)}) custom-call(bf16[8,40,2048]{2,1,0:T(8,128)(2,1)} %bitcast.56, bf16[8,128,40]{2,1,0:T(8,128)(2,1)} %fusion.26.comb_ref, bf16[128,256]{1,0:T(8,128)(2,1)} %get-tuple-element.21.act_ref), custom_call_target="tpu_custom_call" | custom-call | tf_op jit(solution)/shard_map/combine/pallas_call | solution.py:245
  92.9 1.4 %fusion.18 = f32[128]{0:T(128)S(1)} fusion(bf16[128,2048]{1,0:T(8,128)(2,1)S(1)} %copy-done.1, bf16[128,2048]{1,0:T(8,128)(2,1)} %get-tuple-element.10, f32[2048]{0:T(1024)S(1)} %copy-done.14, f32[128]{0:T(128)S(1)} %add_rsqrt_fusion), kind=kLoop, calls=%fused_computation.27 | loop fusion | flops 1572736 | bytes 1057792 | tf_op jit(solution)/shard_map/reduce_sum | solution.py:465
  94.3 1.6 %fusion.22 = bf16[128,2048]{1,0:T(8,128)(2,1)S(1)} fusion(bf16[128,2048]{1,0:T(8,128)(2,1)S(1)} %copy-done.1, bf16[128,2048]{1,0:T(8,128)(2,1)} %get-tuple-element.10, bf16[128,2048]{1,0:T(8,128)(2,1)} %param.16, f32[128]{0:T(128)S(1)} %broadcast_multiply_fusion, f32[2048]{0:T(1024)S(1)} %copy-done.14, f32[128]{0:T(128)S(1)} %add_rsqrt_fusion), kind=kLoop, calls=%fused_computation.31 | loop fusion | flops 2621440 | bytes 2106368 | tf_op jit(solution)/shard_map/convert_element_type | solution.py:467
  95.9 0.3 copy.32
  96.2 1.0 copy.33
  97.2 2.2 %fusion.16.d_in_ref = f32[128,256]{1,0:T(8,128)} fusion(bf16[128,2048]{1,0:T(8,128)(2,1)S(1)} %fusion.22, bf16[2048,256]{1,0:T(8,128)(2,1)} %param.24, f32[256]{0:T(256)S(1)} %copy-done.16, f32[128]{0:T(128)S(1)} %copy-done.15, f32[128]{0:T(128)S(1)} %copy-done.17, bf16[128,256]{1,0:T(8,128)(2,1)S(1)} %copy-done.11), kind=kOutput, calls=%fused_computation.24 | convolution fusion | flops 134643712 | bytes 1771520 | tf_op jit(solution)/shard_map/dot_general | solution.py:468
  99.5 0.7 copy.34.rstd_ref
  100.2 19.0 %finish.1 = (bf16[8,128,256]{2,1,0:T(8,128)(2,1)}, f32[128,256]{1,0:T(8,128)}) custom-call(bf16[8,128,256]{2,1,0:T(8,128)(2,1)} %bitcast.57, f32[128,256]{1,0:T(8,128)} %fusion.16.d_in_ref, f32[128,256]{1,0:T(8,128)} %get-tuple-element.20.norm_in_ref, f32[128,1]{1,0:T(8,128)} %copy.34.rstd_ref, f32[31,256]{1,0:T(8,128)} %taps_ref.1), custom_call_target="tpu_custom_call" | custom-call | tf_op jit(solution)/shard_map/finish/pallas_call | solution.py:358
  119.2 2.2 %convolution_bitcast_fusion = f32[256,256]{1,0:T(8,128)} fusion(bf16[8,128,256]{2,1,0:T(8,128)(2,1)} %get-tuple-element.11, bf16[8,128,256]{2,1,0:T(8,128)(2,1)} %get-tuple-element.12), kind=kOutput, calls=%fused_computation.21 | convolution fusion | flops 134217728 | bytes 1310720 | tf_op jit(solution)/shard_map/dot_general | solution.py:17
  121.4 1.6 %multiply_convert_fusion.5 = (bf16[128,256]{1,0:T(8,128)(2,1)}, bf16[128,256]{1,0:T(8,128)(2,1)}) fusion(f32[128,256]{1,0:T(8,128)} %get-tuple-element.13, bf16[128,256]{1,0:T(8,128)(2,1)S(1)} %copy-done.12, bf16[128,256]{1,0:T(8,128)(2,1)S(1)} %copy-done.13), kind=kLoop, calls=%fused_computation.53 | loop fusion | flops 393216 | bytes 393216 | tf_op jit(solution)/shard_map/convert_element_type | solution.py:477
  123.1 4.1 %fusion.2 = bf16[1,512,2048]{2,1,0:T(8,128)(2,1)} fusion(bf16[320,2048]{1,0:T(8,128)(2,1)S(1)} %bitcast.64, f32[320,512]{1,0:T(8,128)} %copy-done.20, f32[320,512]{1,0:T(8,128)} %copy-done.19), kind=kOutput, calls=%fused_computation.6 | convolution fusion | flops 673120256 | bytes 4718592 | tf_op jit(solution)/shard_map/dot_general | solution.py:17
  127.1 2.6 %fusion.1 = bf16[1,2048,512]{2,1,0:T(8,128)(2,1)} fusion(bf16[320,2048]{1,0:T(8,128)(2,1)S(1)} %bitcast.61, bf16[320,512]{1,0:T(8,128)(2,1)S(1)} %copy-done.10), kind=kOutput, calls=%fused_computation.5 | convolution fusion | flops 672137216 | bytes 3735552 | tf_op jit(solution)/shard_map/dot_general | solution.py:17
  129.8 2.6 %fusion = bf16[1,2048,512]{2,1,0:T(8,128)(2,1)} fusion(bf16[320,2048]{1,0:T(8,128)(2,1)S(1)} %bitcast.62, bf16[320,512]{1,0:T(8,128)(2,1)S(1)} %copy-done.8), kind=kOutput, calls=%fused_computation.4 | convolution fusion | flops 672137216 | bytes 3735552 | tf_op jit(solution)/shard_map/dot_general | solution.py:17
  (35 shorter events, 0.1 us)
Async XLA Ops:
  0.6 48.0 %copy-start = (bf16[1,2048,512]{2,1,0:T(8,128)(2,1)S(1)}, bf16[1,2048,512]{2,1,0:T(8,128)(2,1)}, u32[]{:S(2)}) copy-start(bf16[1,2048,512]{2,1,0:T(8,128)(2,1)} %param.21) | copy-start | bytes 6291460
  48.6 1.1 copy-start.3
  48.6 3.4 %copy-start.5 = (bf16[1,8,40,2048]{3,2,1,0:T(8,128)(2,1)}, bf16[1,8,40,2048]{3,2,1,0:T(8,128)(2,1)S(1)}, u32[]{:S(2)}) copy-start(bf16[1,8,40,2048]{3,2,1,0:T(8,128)(2,1)S(1)} %get-tuple-element.14) | copy-start | bytes 3932164
  48.6 2.5 %copy-start.2 = (bf16[1,2048,512]{2,1,0:T(8,128)(2,1)S(1)}, bf16[1,2048,512]{2,1,0:T(8,128)(2,1)}, u32[]{:S(2)}) copy-start(bf16[1,2048,512]{2,1,0:T(8,128)(2,1)} %param.22) | copy-start | bytes 6291460
  51.1 0.9 copy-start.19
  51.1 1.9 %copy-start.18 = (bf16[1,512,2048]{2,1,0:T(8,128)(2,1)S(1)}, bf16[1,512,2048]{2,1,0:T(8,128)(2,1)}, u32[]{:S(2)}) copy-start(bf16[1,512,2048]{2,1,0:T(8,128)(2,1)} %param.23) | copy-start | bytes 6291460
  52.0 2.1 %copy-start.20 = (f32[320,512]{1,0:T(8,128)}, f32[320,512]{1,0:T(8,128)S(1)}, u32[]{:S(2)}) copy-start(f32[320,512]{1,0:T(8,128)S(1)} %fusion.9) | copy-start | bytes 1966084
  54.1 0.9 copy-start.7
  54.1 0.9 copy-start.9
  55.0 2.9 %copy-start.11 = (bf16[128,256]{1,0:T(8,128)(2,1)S(1)}, bf16[128,256]{1,0:T(8,128)(2,1)}, u32[]{:S(2)}) copy-start(bf16[128,256]{1,0:T(8,128)(2,1)} %param.25) | copy-start | bytes 196612
  55.0 2.9 %copy-start.15 = (f32[128]{0:T(128)S(1)}, f32[128]{0:T(128)}, u32[]{:S(2)}) copy-start(f32[128]{0:T(128)} %param.27) | copy-start | bytes 1540
  55.0 2.9 %copy-start.16 = (f32[256]{0:T(256)S(1)}, f32[256]{0:T(256)}, u32[]{:S(2)}) copy-start(f32[256]{0:T(256)} %param.28) | copy-start | bytes 3076
  55.0 2.9 %copy-start.17 = (f32[128]{0:T(128)S(1)}, f32[128]{0:T(128)}, u32[]{:S(2)}) copy-start(f32[128]{0:T(128)} %param.26) | copy-start | bytes 1540
  57.0 36.0 %copy-start.1 = (bf16[128,2048]{1,0:T(8,128)(2,1)S(1)}, bf16[128,2048]{1,0:T(8,128)(2,1)}, u32[]{:S(2)}) copy-start(bf16[128,2048]{1,0:T(8,128)(2,1)} %param.17) | copy-start | bytes 1572868
  57.0 36.0 %copy-start.14 = (f32[2048]{0:T(1024)S(1)}, f32[2048]{0:T(1024)}, u32[]{:S(2)}) copy-start(f32[2048]{0:T(1024)} %param.18) | copy-start | bytes 24580
  97.2 24.2 %copy-start.12 = (bf16[128,256]{1,0:T(8,128)(2,1)S(1)}, bf16[128,256]{1,0:T(8,128)(2,1)}, u32[]{:S(2)}) copy-start(bf16[128,256]{1,0:T(8,128)(2,1)} %param.30) | copy-start | bytes 196612
  97.2 24.2 %copy-start.13 = (bf16[128,256]{1,0:T(8,128)(2,1)S(1)}, bf16[128,256]{1,0:T(8,128)(2,1)}, u32[]{:S(2)}) copy-start(bf16[128,256]{1,0:T(8,128)(2,1)} %param.31) | copy-start | bytes 196612
  99.5 23.6 %copy-start.6 = (bf16[1,8,40,2048]{3,2,1,0:T(8,128)(2,1)S(1)}, bf16[1,8,40,2048]{3,2,1,0:T(8,128)(2,1)}, u32[]{:S(2)}) copy-start(bf16[1,8,40,2048]{3,2,1,0:T(8,128)(2,1)} %copy-done.5) | copy-start | bytes 3932164
  123.1 4.1 %copy-start.4 = (bf16[1,8,40,2048]{3,2,1,0:T(8,128)(2,1)S(1)}, bf16[1,8,40,2048]{3,2,1,0:T(8,128)(2,1)}, u32[]{:S(2)}) copy-start(bf16[1,8,40,2048]{3,2,1,0:T(8,128)(2,1)} %copy-done.3) | copy-start | bytes 3932164
  123.1 4.1 %copy-start.10 = (bf16[320,512]{1,0:T(8,128)(2,1)S(1)}, bf16[320,512]{1,0:T(8,128)(2,1)}, u32[]{:S(2)}) copy-start(bf16[320,512]{1,0:T(8,128)(2,1)} %copy-done.9) | copy-start | bytes 983044
  127.1 2.6 %copy-start.8 = (bf16[320,512]{1,0:T(8,128)(2,1)S(1)}, bf16[320,512]{1,0:T(8,128)(2,1)}, u32[]{:S(2)}) copy-start(bf16[320,512]{1,0:T(8,128)(2,1)} %copy-done.7) | copy-start | bytes 983044
